TPU v7x, 32 devices: a whole 2x2x4 slice. The times are simulated.
32 devices in a mesh: fs: 8 (over z, x), tp: 4 (over y, core).
Axes of the slice: x: 2, y: 2, z: 4, core: 2. Of those that a mesh axis runs over, the one named last changes fastest.
Arguments:
- normed_input: bfloat16 [5120, 2048], P('fs'), may hold values from -448 to 448
- key_cotangent: bfloat16 [5120, 512], P('fs', 'tp'), may hold values from -0.078125 to 0.078125
- value_cotangent: bfloat16 [5120, 1024], P('fs', 'tp'), may hold values from -0.078125 to 0.078125
- key_factor: bfloat16 [512, 128], P('tp'), may hold values from -2.8 to 2.8
- value_factor: bfloat16 [1024, 128], P('tp'), may hold values from -2.8 to 2.8
- key_weight: float32 [2048, 512], P('fs', 'tp'), may hold values from -0.125 to 0.125
- value_weight: float32 [2048, 1024], P('fs', 'tp'), may hold values from -0.125 to 0.125
- first_moments: float32 [2, 2048, 128], P(None, 'fs', 'tp'), may hold values from -0.6 to 0.6
- second_moments: float32 [2, 2048, 128], P(None, 'fs', 'tp'), may hold values from 0.001 to 0.1
Outputs:
- first_new: float32 [2, 2048, 128], P(None, 'fs', 'tp')
- second_new: float32 [2, 2048, 128], P(None, 'fs', 'tp')
- new_key_weight: float32 [2048, 512], P('fs', 'tp')
- new_value_weight: float32 [2048, 1024], P('fs', 'tp')
- key_copy: bfloat16 [2048, 512], P(None, 'tp')
- value_copy: bfloat16 [2048, 1024], P(None, 'tp')
All inputs are finite; a program needn't handle non-finite values.
Results may differ from a plain program's by a relative error of at most 0.005.
Values may be sent and summed in bfloat16 or wider, within the bound.
A program may use at most 64 MiB of HBM per device.

v0:
```python
import jax
import jax.numpy as jnp
from jax import lax
from jax.sharding import PartitionSpec as P

D = 2048
RANK = 128


step_rate = 0.05
clip_target = 0.1
beta_first = 0.8
beta_second = 0.95
small_eps = 1e-08
norm_eps = 1e-06


def split_product(normed_input, reduced):
    upper = reduced.astype(jnp.bfloat16)
    lower = (reduced - upper.astype(jnp.float32)).astype(jnp.bfloat16)
    joined = jnp.concatenate([upper, lower], axis=1)
    width = reduced.shape[1]
    both = lax.dot_general(
        normed_input, joined, (((0,), (0,)), ((), ())), preferred_element_type=jnp.float32
    )
    return both[:, :width] + both[:, width:]


def local(
    normed_input,
    key_cotangent,
    value_cotangent,
    key_factor,
    value_factor,
    key_weight,
    value_weight,
    first_moments,
    second_moments,
):
    rank_total = key_factor.shape[1]
    rank_dev = first_moments.shape[2]
    tok_rows = normed_input.shape[0]
    highest = lax.Precision.HIGHEST
    group_count = lax.axis_size("tp")
    key_reduced = jnp.dot(key_cotangent, key_factor, preferred_element_type=jnp.float32)
    value_reduced = jnp.dot(value_cotangent, value_factor, preferred_element_type=jnp.float32)
    arranged = jnp.stack(
        [
            key_reduced.reshape(tok_rows, group_count, rank_dev),
            value_reduced.reshape(tok_rows, group_count, rank_dev),
        ],
        axis=2,
    )
    arranged = arranged.reshape(tok_rows, 2 * rank_total)
    own_reduced = lax.psum_scatter(arranged, "tp", scatter_dimension=1, tiled=True)
    own_terms = lax.psum_scatter(
        split_product(normed_input, own_reduced), "fs", scatter_dimension=0, tiled=True
    )
    own_key = own_terms[:, :rank_dev]
    own_value = own_terms[:, rank_dev:]
    proj_key, proj_value = (own_key, own_value)
    projected = jnp.stack([proj_key, proj_value])
    prior_first, prior_second = (first_moments, second_moments)
    total_sq = lax.psum(jnp.sum(projected * projected), ("fs", "tp"))
    clip_limit = clip_target * jnp.sqrt(jnp.float32(2 * D * RANK))
    clip_factor = jnp.minimum(1.0, clip_limit / jnp.sqrt(total_sq + norm_eps))
    scaled = clip_factor * projected
    first_new = beta_first * prior_first + (1.0 - beta_first) * scaled
    second_new = beta_second * prior_second + (1.0 - beta_second) * scaled * scaled
    direction = first_new / (jnp.sqrt(second_new) + small_eps)
    full_direction = lax.all_gather(direction, "tp", axis=2, tiled=True)
    first_out, second_out = (first_new, second_new)
    back = (((1,), (1,)), ((), ()))
    update_key = lax.dot_general(
        full_direction[0], key_factor.astype(jnp.float32), back, precision=highest
    )
    update_value = lax.dot_general(
        full_direction[1], value_factor.astype(jnp.float32), back, precision=highest
    )
    new_key = key_weight - step_rate * update_key
    new_value = value_weight - step_rate * update_value
    key_copy, value_copy = (
        lax.all_gather(new_key.astype(jnp.bfloat16), "fs", axis=0, tiled=True),
        lax.all_gather(new_value.astype(jnp.bfloat16), "fs", axis=0, tiled=True),
    )
    return (first_out, second_out, new_key, new_value, key_copy, value_copy)


def solution(mesh):
    placed = (
        P("fs", None),
        P("fs", "tp"),
        P("fs", "tp"),
        P("tp", None),
        P("tp", None),
        P("fs", "tp"),
        P("fs", "tp"),
        P(None, "fs", "tp"),
        P(None, "fs", "tp"),
    )
    return jax.shard_map(
        local,
        mesh=mesh,
        in_specs=placed,
        out_specs=(
            P(None, "fs", "tp"),
            P(None, "fs", "tp"),
            P("fs", "tp"),
            P("fs", "tp"),
            P(None, "tp"),
            P(None, "tp"),
        ),
        check_vma=False,
    )
```

profile of v0, /device:TPU:0, one launch (start us, length us, event | category | flops | bytes accessed | tf_op | source)
XLA Modules:
  0.0 204.1 jit_solution(474494371642411430)
XLA Ops:
  7.2 0.0 copy-start
  7.2 0.0 reduce-scatter.3.cloned.1.call-start
  7.2 1.3 fusion.10
  8.5 1.2 fusion.11
  9.8 0.9 pad_maximum_fusion
  10.6 0.0 reduce-scatter.3.cloned.1.call-update
  10.7 0.0 reduce-scatter.5.cloned.1.call-start
  10.7 25.5 %reduce-scatter.3.cloned.1.call-done = f32[640,64]{0,1:T(8,128)} async-done(((f32[640,256]{0,1:T(8,128)}), f32[640,64]{0,1:T(8,128)}) %reduce-scatter.3.cloned.1.call-update) | async-done | bytes 163856 | tf_op jit(solution)/shard_map/reduce_scatter | solution.py:55
  36.3 1.0 subtract_convert_fusion
  37.3 0.0 copy-done
  37.3 0.0 copy-start.5
  37.3 0.0 copy-start.6
  37.3 0.0 copy-start.1
  37.3 0.0 copy-start.2
  37.3 0.6 convolution_bitcast_fusion
  37.9 0.0 copy-start.3
  37.9 0.0 copy-start.4
  37.9 0.8 slice_add_fusion
  38.8 0.0 reduce-scatter.5.cloned.1.call-update
  38.8 0.0 all-gather.2.cloned.1.call-start
  38.9 64.4 %reduce-scatter.5.cloned.1.call-done = f32[256,64]{0,1:T(8,128)} async-done(((f32[2048,64]{0,1:T(8,128)}), f32[256,64]{0,1:T(8,128)}) %reduce-scatter.5.cloned.1.call-update) | async-done | bytes 65552 | tf_op jit(solution)/shard_map/reduce_scatter | solution.py:56
  103.2 0.8 slice_bitcast_fusion.5
  104.0 0.6 multiply_reduce_fusion
  104.6 40.3 %psum.7 = f32[]{:T(128)} all-reduce(f32[]{:T(128)} %multiply_reduce_fusion), channel_id=1, replica_groups=mesh['fs'=8,'tp'=4] {'fs','tp'}, use_global_device_ids=true, to_apply=%region_3.0 | all-reduce | flops 1 | bytes 8 | tf_op jit(solution)/shard_map/psum | solution.py:64
  145.6 0.0 copy-done.5
  145.6 0.0 copy-done.6
  145.6 0.7 add_divide_fusion
  146.3 6.7 %all_gather.9 = f32[2,256,128]{1,2,0:T(8,128)S(1)} all-gather(f32[2,256,32]{1,2,0:T(8,128)S(1)} %get-tuple-element.6), channel_id=1, replica_groups=mesh['fs'=8,'tp'=4] {'tp'}, dimensions={2}, use_global_device_ids=true | all-gather | bytes 327680 | tf_op jit(solution)/shard_map/all_gather | solution.py:71
  153.0 0.0 copy-done.1
  153.0 0.0 copy-done.2
  153.0 1.1 fusion.9
  154.0 0.0 all-gather.2.cloned.1.call-update
  154.1 0.0 copy-done.3
  154.1 0.0 copy-done.4
  154.1 0.9 fusion.8
  155.0 32.1 %all_gather.10 = bf16[2048,128]{1,0:T(8,128)(2,1)S(1)} all-gather(bf16[256,128]{1,0:T(8,128)(2,1)S(1)} %get-tuple-element.13), channel_id=1, replica_groups=mesh['fs'=8,'tp'=4] {'fs'}, dimensions={0}, use_global_device_ids=true | all-gather | bytes 589824 | tf_op jit(solution)/shard_map/all_gather | solution.py:83
  187.2 7.3 %all-gather.2.cloned.1.call-done = bf16[2048,256]{1,0:T(8,128)(2,1)} async-done(((bf16[256,256]{1,0:T(8,128)(2,1)}), bf16[2048,256]{1,0:T(8,128)(2,1)}) %all-gather.2.cloned.1.call-update) | async-done | bytes 1048592 | tf_op jit(solution)/shard_map/all_gather | solution.py:84
  194.5 0.8 copy.19
  195.3 2.3 %copy.20 = bf16[2048,256]{1,0:T(8,128)(2,1)} copy(bf16[2048,256]{1,0:T(8,128)(2,1)} %all-gather.2.cloned.1.call-done) | data formatting | bytes 2097152
Async XLA Ops:
  7.2 30.1 %copy-start = (bf16[640,2048]{1,0:T(8,128)(2,1)S(1)}, bf16[640,2048]{1,0:T(8,128)(2,1)}, u32[]{:S(2)}) copy-start(bf16[640,2048]{1,0:T(8,128)(2,1)} %param.9) | copy-start | bytes 7864324
  7.2 29.1 %reduce-scatter.3.cloned.1.call-start = ((), (), s32[]{:S(2)}) async-start(), calls=%async_computation.2 | async-start | bytes 819200 | tf_op jit(solution)/shard_map/reduce_scatter | solution.py:55
  10.7 92.5 %reduce-scatter.5.cloned.1.call-start = ((), (), s32[]{:S(2)}) async-start(), calls=%async_computation.3 | async-start | bytes 589824 | tf_op jit(solution)/shard_map/reduce_scatter | solution.py:56
  37.3 108.3 %copy-start.5 = (f32[2,256,32]{1,2,0:T(8,128)S(1)}, f32[2,256,32]{1,2,0:T(8,128)}, u32[]{:S(2)}) copy-start(f32[2,256,32]{1,2,0:T(8,128)} %param.17) | copy-start | bytes 196612
  37.3 108.3 %copy-start.6 = (f32[2,256,32]{1,2,0:T(8,128)S(1)}, f32[2,256,32]{1,2,0:T(8,128)}, u32[]{:S(2)}) copy-start(f32[2,256,32]{1,2,0:T(8,128)} %param.16) | copy-start | bytes 196612
  37.3 115.7 %copy-start.1 = (f32[256,256]{1,0:T(8,128)S(1)}, f32[256,256]{1,0:T(8,128)}, u32[]{:S(2)}) copy-start(f32[256,256]{1,0:T(8,128)} %param.15) | copy-start | bytes 786436
  37.3 115.7 %copy-start.2 = (bf16[256,128]{1,0:T(8,128)(2,1)S(1)}, bf16[256,128]{1,0:T(8,128)(2,1)}, u32[]{:S(2)}) copy-start(bf16[256,128]{1,0:T(8,128)(2,1)} %param.13) | copy-start | bytes 196612
  37.9 116.2 %copy-start.3 = (f32[256,128]{1,0:T(8,128)S(1)}, f32[256,128]{1,0:T(8,128)}, u32[]{:S(2)}) copy-start(f32[256,128]{1,0:T(8,128)} %param.14) | copy-start | bytes 393220
  37.9 116.2 %copy-start.4 = (bf16[128,128]{1,0:T(8,128)(2,1)S(1)}, bf16[128,128]{1,0:T(8,128)(2,1)}, u32[]{:S(2)}) copy-start(bf16[128,128]{1,0:T(8,128)(2,1)} %param.12) | copy-start | bytes 98308
  38.8 155.7 %all-gather.2.cloned.1.call-start = ((), (), s32[]{:S(2)}) async-start(), calls=%async_computation.4 | async-start | bytes 1179648 | tf_op jit(solution)/shard_map/all_gather | solution.py:84
Sparse Core Ops, SparseCore 0:
  11.1 25.1 reduce-scatter.2
  40.2 63.0 reduce-scatter.4
  154.2 40.2 all-gather.1
where the time goes:
time: 204 us
  waiting for transfers between devices  97.2 us (48%)
  blocking collectives  79.1 us (39%)
  between operations  14.5 us (7%)
  matrix products  5.11 us (3%)
  other arithmetic  4.06 us (2%)
  local copies, waits for them, and re-layouts  3.88 us (2%)
    reduce_scatter x1, waiting for transfers between devices, local(): lax.psum_scatter(split_product(normed_input, own_reduced), 'fs', scatter_...  64.4 us
    psum x1, blocking collectives, local(): total_sq = lax.psum(jnp.sum(projected * projected), ('fs', 'tp'))  40.3 us
    all_gather x1, blocking collectives, local(): lax.all_gather(new_key.astype(jnp.bfloat16), 'fs', axis=0, tiled=True)  32.1 us
    reduce_scatter x1, waiting for transfers between devices, local(): lax.psum_scatter(arranged, 'tp', scatter_dimension=1, tiled=True)  25.5 us
    all_gather x1, waiting for transfers between devices, local(): lax.all_gather(new_value.astype(jnp.bfloat16), 'fs', axis=0, tiled=True)  7.3 us
    all_gather x1, blocking collectives, local(): full_direction = lax.all_gather(direction, 'tp', axis=2, tiled=True)  6.71 us
  transfers between devices with their start and end apart: 3, of which 3 were waited for; matrix products, arithmetic and copies ran while one was open for 0% of the time, Pallas kernels for 0%

commit v1 on v0

v1 whole, which is shorter than its diff:
```python
import functools

import jax
import jax.numpy as jnp
from jax import lax
from jax.experimental import pallas as pl
from jax.experimental.pallas import tpu as pltpu
from jax.sharding import PartitionSpec as P

step_rate = 0.05
clip_target = 0.1
beta_first = 0.8
beta_second = 0.95
small_eps = 1e-08
norm_eps = 1e-06

MESH = pl.DeviceIdType.MESH
BF16 = jnp.bfloat16
F32 = jnp.float32


def flip(a):
    return jnp.transpose(a.astype(F32))


def kernel(
    n_fs,
    n_tp,
    x_hbm,
    dk_ref,
    dv_ref,
    kf_ref,
    vf_ref,
    wk_ref,
    wv_ref,
    fm_ref,
    sm_ref,
    first_ref,
    second_ref,
    newk_ref,
    newv_ref,
    kcopy_ref,
    vcopy_ref,
    x_ref,
    part_ref,
    partin_ref,
    tok_ref,
    tokin_ref,
    sq_ref,
    sqin_ref,
    gat_ref,
    wall_ref,
    x_sem,
    part_ss,
    part_rs,
    tok_ss,
    tok_rs,
    sq_ss,
    sq_rs,
    gf_ss,
    gf_rs,
    gt_ss,
    gt_rs,
    w_ss,
    w_rs,
    wx_ss,
    wx_rs,
):
    fs = lax.axis_index("fs")
    tp = lax.axis_index("tp")
    n_dev = n_fs * n_tp
    lin = fs * n_tp + tp
    rank = kf_ref.shape[1]
    r = rank // n_tp
    rows = wk_ref.shape[0]
    nk = wk_ref.shape[1]
    nv = wv_ref.shape[1]
    model = x_ref.shape[1]
    pair = 2 if n_fs % 2 == 0 else 1
    n_far = n_fs // pair
    far = fs // pair
    near = fs % pair

    x_copy = pltpu.make_async_copy(x_hbm, x_ref, x_sem)
    x_copy.start()

    barrier = pltpu.get_barrier_semaphore()

    @pl.loop(1, n_dev)
    def _(k):
        other = lax.rem(lin + k, n_dev)
        pl.semaphore_signal(
            barrier,
            inc=1,
            device_id={"fs": other // n_tp, "tp": lax.rem(other, n_tp)},
            device_id_type=MESH,
        )

    kft = flip(kf_ref[...]).astype(BF16)
    vft = flip(vf_ref[...]).astype(BF16)
    last = (((1,), (1,)), ((), ()))
    red_k = lax.dot_general(kft, dk_ref[...], last, preferred_element_type=F32)
    red_v = lax.dot_general(vft, dv_ref[...], last, preferred_element_type=F32)
    for j in range(n_tp):
        part_ref[j, :r, :] = red_k[j * r : (j + 1) * r].astype(BF16)
        part_ref[j, r:, :] = red_v[j * r : (j + 1) * r].astype(BF16)
    wall_ref[fs, :, :nk] = wk_ref[...].astype(BF16)
    wall_ref[fs, :, nk:] = wv_ref[...].astype(BF16)

    pl.semaphore_wait(barrier, n_dev - 1)

    def part_copy(k):
        to = lax.rem(tp + k, n_tp)
        return pltpu.make_async_remote_copy(
            src_ref=part_ref.at[to],
            dst_ref=partin_ref.at[k - 1],
            send_sem=part_ss.at[k - 1],
            recv_sem=part_rs.at[k - 1],
            device_id={"tp": to},
            device_id_type=MESH,
        )

    parts = [part_copy(k) for k in range(1, n_tp)]
    for c in parts:
        c.start()

    def wall_copy(k):
        to = lax.rem(far + k, n_far) * pair + near
        return pltpu.make_async_remote_copy(
            src_ref=wall_ref.at[fs],
            dst_ref=wall_ref.at[fs],
            send_sem=w_ss.at[k - 1],
            recv_sem=w_rs.at[k - 1],
            device_id={"fs": to},
            device_id_type=MESH,
        )

    def wall_in(k):
        origin = lax.rem(far + n_far - k, n_far) * pair + near
        return pltpu.make_async_copy(
            wall_ref.at[origin], wall_ref.at[origin], w_rs.at[k - 1]
        )

    def wall_pair(k):
        block = lax.rem(far + n_far - k, n_far) * pair + near
        return pltpu.make_async_remote_copy(
            src_ref=wall_ref.at[block],
            dst_ref=wall_ref.at[block],
            send_sem=wx_ss.at[k],
            recv_sem=wx_rs.at[k],
            device_id={"fs": far * pair + 1 - near},
            device_id_type=MESH,
        )

    walls = [wall_copy(k) for k in range(1, n_far)]
    for c in walls:
        c.start()
    pairs = []
    if pair == 2:
        pairs.append(wall_pair(0))
        pairs[-1].start()

    fmt = jnp.concatenate([flip(fm_ref[0]), flip(fm_ref[1])], axis=0)
    smt = jnp.concatenate([flip(sm_ref[0]), flip(sm_ref[1])], axis=0)

    for c in parts:
        c.wait_recv()
    own = part_ref[tp].astype(F32)
    for k in range(1, n_tp):
        own = own + partin_ref[k - 1].astype(F32)
    own = own.astype(BF16)
    x_copy.wait()

    def tok_copy(c):
        return pltpu.make_async_remote_copy(
            src_ref=tok_ref.at[c],
            dst_ref=tokin_ref.at[fs],
            send_sem=tok_ss.at[c],
            recv_sem=tok_rs.at[fs],
            device_id={"fs": c},
            device_id_type=MESH,
        )

    width = max(rows, min(256, model))
    for base in range(0, model, width):
        prod = lax.dot_general(
            own,
            x_ref[:, base : base + width],
            (((1,), (0,)), ((), ())),
            preferred_element_type=F32,
        )
        for c in range(base // rows, (base + width) // rows):
            at = c * rows - base
            tok_ref[c] = prod[:, at : at + rows].astype(BF16)

            @pl.when(c != fs)
            def _():
                tok_copy(c).start()

    total = tok_ref[fs].astype(F32)
    for k in range(1, n_fs):
        origin = lax.rem(fs + k, n_fs)
        pltpu.make_async_copy(
            tokin_ref.at[origin], tokin_ref.at[origin], tok_rs.at[origin]
        ).wait()
        total = total + tokin_ref[origin].astype(F32)

    sq_ref[...] = jnp.full(sq_ref.shape, jnp.sum(total * total), F32)

    def sq_copy(k):
        other = lax.rem(lin + k, n_dev)
        return pltpu.make_async_remote_copy(
            src_ref=sq_ref,
            dst_ref=sqin_ref.at[k - 1],
            send_sem=sq_ss,
            recv_sem=sq_rs,
            device_id={"fs": other // n_tp, "tp": lax.rem(other, n_tp)},
            device_id_type=MESH,
        )

    @pl.loop(1, n_dev)
    def _(k):
        sq_copy(k).start()

    pltpu.make_async_copy(sqin_ref, sqin_ref, sq_rs).wait()
    total_sq = jnp.max(jnp.sum(sqin_ref[...], axis=0) + sq_ref[...])
    limit = clip_target * (2.0 * model * rank) ** 0.5
    clip_factor = jnp.minimum(
        1.0, limit / jnp.sqrt(jnp.full((1, 1), total_sq + norm_eps, F32))
    )
    scaled = clip_factor * total
    first_new = beta_first * fmt + (1.0 - beta_first) * scaled
    second_new = beta_second * smt + (1.0 - beta_second) * scaled * scaled
    direction = first_new / (jnp.sqrt(second_new) + small_eps)

    mine = pl.ds(pl.multiple_of(tp * r, r), r)
    gat_ref[fs, 0, mine, :] = direction[:r].astype(BF16)
    gat_ref[fs, 1, mine, :] = direction[r:].astype(BF16)

    def gat_copy(k):
        block = gat_ref.at[fs, :, mine, :]
        return pltpu.make_async_remote_copy(
            src_ref=block,
            dst_ref=block,
            send_sem=gf_ss.at[k - 1],
            recv_sem=gf_rs.at[k - 1],
            device_id={"fs": lax.rem(fs + k, n_fs)},
            device_id_type=MESH,
        )

    def gat_in(k):
        origin = lax.rem(fs + n_fs - k, n_fs)
        block = gat_ref.at[origin, :, mine, :]
        return pltpu.make_async_copy(block, block, gf_rs.at[k - 1])

    bits = []
    b = n_tp // 2
    while b:
        bits.append(b)
        b //= 2

    def flipped(v, bit):
        return v + bit - 2 * bit * (v // bit % 2)

    held = [[]]
    for bit in bits:
        held.append(held[-1] + [bit])

    def sources(step):
        out = [0]
        for bit in bits[:step]:
            out = out + [o + bit for o in out]
        return out

    def tp_of(mask):
        v = tp
        for bit in bits:
            if mask & bit:
                v = flipped(v, bit)
        return v

    def share_copy(k, step, mask):
        origin = lax.rem(fs + n_fs - k, n_fs)
        at = pl.ds(pl.multiple_of(tp_of(mask) * r, r), r)
        block = gat_ref.at[origin, :, at, :]
        slot = mask | bits[step]
        return pltpu.make_async_remote_copy(
            src_ref=block,
            dst_ref=block,
            send_sem=gt_ss.at[k, slot - 1],
            recv_sem=gt_rs.at[k, slot - 1],
            device_id={"tp": flipped(tp, bits[step])},
            device_id_type=MESH,
        )

    def share_in(k, slot):
        origin = lax.rem(fs + n_fs - k, n_fs)
        at = pl.ds(pl.multiple_of(tp_of(slot) * r, r), r)
        block = gat_ref.at[origin, :, at, :]
        return pltpu.make_async_copy(block, block, gt_rs.at[k, slot - 1])

    shares = []

    def share(k, step):
        for mask in sources(step):
            c = share_copy(k, step, mask)
            c.start()
            shares.append(c)

    gats = [gat_copy(k) for k in range(1, n_fs)]
    if bits:
        share(0, 0)
    for c in gats:
        c.start()

    for i in range(2):
        first_ref[i] = jnp.transpose(first_new[i * r : (i + 1) * r])
        second_ref[i] = jnp.transpose(second_new[i * r : (i + 1) * r])

    for k in range(1, n_far):
        wall_in(k).wait()
        if pair == 2:
            pairs.append(wall_pair(k))
            pairs[-1].start()

    order = list(range(n_fs))
    for k in order:
        if k:
            gat_in(k).wait()
            if bits:
                share(k, 0)
    for step in range(1, len(bits)):
        for k in order:
            for mask in sources(step - 1):
                share_in(k, mask | bits[step - 1]).wait()
            share(k, step)

    back = (((0,), (0,)), ((), ()))

    def update(block):
        up_k = lax.dot_general(gat_ref[block, 0], kft, back, preferred_element_type=F32)
        up_v = lax.dot_general(gat_ref[block, 1], vft, back, preferred_element_type=F32)
        return step_rate * up_k, step_rate * up_v

    for k in range(n_fs):
        origin = lax.rem(fs + n_fs - k, n_fs)
        if bits:
            for mask in sources(len(bits) - 1):
                share_in(k, mask | bits[-1]).wait()
        up_k, up_v = update(origin)
        at = pl.ds(pl.multiple_of(origin * rows, rows), rows)
        if k == 0:
            new_k = wk_ref[...] - up_k
            new_v = wv_ref[...] - up_v
            newk_ref[...] = new_k
            newv_ref[...] = new_v
            kcopy_ref[at, :] = new_k.astype(BF16)
            vcopy_ref[at, :] = new_v.astype(BF16)
        else:
            if k == 1:
                for m in range(n_far if pair == 2 else 0):
                    block = lax.rem(far + n_far - m, n_far) * pair + 1 - near
                    pltpu.make_async_copy(
                        wall_ref.at[block], wall_ref.at[block], wx_rs.at[m]
                    ).wait()
            kcopy_ref[at, :] = (wall_ref[origin, :, :nk].astype(F32) - up_k).astype(BF16)
            vcopy_ref[at, :] = (wall_ref[origin, :, nk:].astype(F32) - up_v).astype(BF16)

    for c in parts + walls + pairs + gats + shares:
        c.wait_send()
    for c in range(n_fs):

        @pl.when(c != fs)
        def _():
            tok_copy(c).wait_send()

    pltpu.make_async_copy(sqin_ref, sqin_ref, sq_ss).wait()


def local(n_fs, n_tp, *args):
    x, dk, dv, kf, vf, wk, wv, fm, sm = args
    tokens, model = x.shape
    rows, nk = wk.shape
    nv = wv.shape[1]
    rank = kf.shape[1]
    r = rank // n_tp
    n_dev = n_fs * n_tp
    dma = pltpu.SemaphoreType.DMA
    vmem = pl.BlockSpec(memory_space=pltpu.VMEM)
    pair = 2 if n_fs % 2 == 0 else 1
    n_far = n_fs // pair
    return pl.pallas_call(
        functools.partial(kernel, n_fs, n_tp),
        out_shape=(
            jax.ShapeDtypeStruct(fm.shape, F32),
            jax.ShapeDtypeStruct(sm.shape, F32),
            jax.ShapeDtypeStruct(wk.shape, F32),
            jax.ShapeDtypeStruct(wv.shape, F32),
            jax.ShapeDtypeStruct((model, nk), BF16),
            jax.ShapeDtypeStruct((model, nv), BF16),
        ),
        in_specs=[pl.BlockSpec(memory_space=pl.ANY)] + [vmem] * 8,
        out_specs=(vmem,) * 6,
        scratch_shapes=[
            pltpu.VMEM((tokens, model), BF16),
            pltpu.VMEM((n_tp, 2 * r, tokens), BF16),
            pltpu.VMEM((max(n_tp - 1, 1), 2 * r, tokens), BF16),
            pltpu.VMEM((n_fs, 2 * r, rows), BF16),
            pltpu.VMEM((n_fs, 2 * r, rows), BF16),
            pltpu.VMEM((8, 128), F32),
            pltpu.VMEM((n_dev - 1, 8, 128), F32),
            pltpu.VMEM((n_fs, 2, rank, rows), BF16),
            pltpu.VMEM((n_fs, rows, nk + nv), BF16),
            dma,
            dma((max(n_tp - 1, 1),)),
            dma((max(n_tp - 1, 1),)),
            dma((n_fs,)),
            dma((n_fs,)),
            dma,
            dma,
            dma((n_fs,)),
            dma((n_fs,)),
            dma((n_fs, n_tp)),
            dma((n_fs, n_tp)),
            dma((n_far,)),
            dma((n_far,)),
            dma((n_far,)),
            dma((n_far,)),
        ],
        compiler_params=pltpu.CompilerParams(
            collective_id=0, has_side_effects=True, vmem_limit_bytes=60 * 1024 * 1024
        ),
    )(*args)


def solution(mesh):
    placed = (
        P("fs", None),
        P("fs", "tp"),
        P("fs", "tp"),
        P("tp", None),
        P("tp", None),
        P("fs", "tp"),
        P("fs", "tp"),
        P(None, "fs", "tp"),
        P(None, "fs", "tp"),
    )
    return jax.shard_map(
        functools.partial(local, mesh.shape["fs"], mesh.shape["tp"]),
        mesh=mesh,
        in_specs=placed,
        out_specs=(
            P(None, "fs", "tp"),
            P(None, "fs", "tp"),
            P("fs", "tp"),
            P("fs", "tp"),
            P(None, "tp"),
            P(None, "tp"),
        ),
        check_vma=False,
    )
```

time: 204 us -> 73.2 us (0.36)
  waiting for transfers between devices: 97.2 us -> 0 us
  blocking collectives: 79.1 us -> 0 us
  Pallas kernels: 0 us -> 59.3 us
  between operations: 14.5 us -> 0.65 us
  local copies, waits for them, and re-layouts: 3.88 us -> 12.9 us
  matrix products: 5.11 us -> 0 us
  other arithmetic: 4.06 us -> 0 us
    reduce_scatter x2 -> x0, waiting for transfers between devices: 89.9 us -> none  [the longest x1 64.4 us: local(): lax.psum_scatter(split_product(normed_input, own_reduced), 'fs', scatter_...]
    pallas_call x0 -> x1, Pallas kernels: none -> 59.3 us  [local(): pl.pallas_call(functools.partial(kernel, n_fs, n_tp), out_shape=(jax.Shap...]
    psum x1 -> x0, blocking collectives: 40.3 us -> none  [local(): total_sq = lax.psum(jnp.sum(projected * projected), ('fs', 'tp'))]
    all_gather x2 -> x0, blocking collectives: 38.8 us -> none  [the longest x1 32.1 us: local(): lax.all_gather(new_key.astype(jnp.bfloat16), 'fs', axis=0, tiled=True)]
    all_gather x1 -> x0, waiting for transfers between devices: 7.3 us -> none  [local(): lax.all_gather(new_value.astype(jnp.bfloat16), 'fs', axis=0, tiled=True)]
    unnamed x16 -> x8, local copies, waits for them, and re-layouts: 3.1 us -> 9.43 us
    dot_general x5 -> x0, matrix products: 5.11 us -> none  [the longest x1 1.3 us: local(): jnp.dot(key_cotangent, key_factor, preferred_element_type=jnp.float32)]
    pallas_call x0 -> x2, local copies, waits for them, and re-layouts: none -> 3.46 us  [local(): pl.pallas_call(functools.partial(kernel, n_fs, n_tp), out_shape=(jax.Shap...]
  transfers between devices with their start and end apart: 3 -> 0, of which waited for: 3 -> 0; matrix products, arithmetic and copies ran while one was open for 0% -> 0% of each run, Pallas kernels for 0% -> 0%
where the time goes in v1:
time: 73.2 us; the launch traced here: 72.8 us
  Pallas kernels  59.3 us (81%)
  local copies, waits for them, and re-layouts  12.9 us (18%)
    pallas_call x1, Pallas kernels, local(): pl.pallas_call(functools.partial(kernel, n_fs, n_tp), out_shape=(jax.Shap...  59.3 us
    unnamed x8, local copies, waits for them, and re-layouts  9.43 us
    pallas_call x2, local copies, waits for them, and re-layouts, local(): pl.pallas_call(functools.partial(kernel, n_fs, n_tp), out_shape=(jax.Shap...  3.46 us

profile of v1, /device:TPU:0, one launch (start us, length us, event | category | flops | bytes accessed | tf_op | source)
XLA Modules:
  0.0 72.8 jit_solution(16854042271370442109)
XLA Ops:
  0.6 1.7 %copy.15.fm_ref = f32[2,256,32]{2,1,0:T(8,128)} copy(f32[2,256,32]{1,2,0:T(8,128)} %param.16) | data formatting | bytes 131072 | tf_op args[7]
  2.3 1.7 %copy.16.sm_ref = f32[2,256,32]{2,1,0:T(8,128)} copy(f32[2,256,32]{1,2,0:T(8,128)} %param.17) | data formatting | bytes 131072 | tf_op args[8]
  4.0 59.3 %shard_map.136 = (f32[2,256,32]{2,1,0:T(8,128)}, f32[2,256,32]{2,1,0:T(8,128)}, f32[256,128]{1,0:T(8,128)}, f32[256,256]{1,0:T(8,128)}, bf16[2048,128]{1,0:T(8,128)(2,1)}, /*index=5*/bf16[2048,256]{1,0:T(8,128)(2,1)}) custom-call(bf16[640,2048]{1,0:T(8,128)(2,1)} %x_hbm.1, bf16[640,128]{1,0:T(8,128)(2,1)} %dk_ref.1, bf16[640,256]{1,0:T(8,128)(2,1)} %dv_ref.1, ...), custom_call_target="tpu_custom_call" | custom-call | tf_op jit(solution)/shard_map/pallas_call | solution.py:392
  63.2 0.0 copy-start
  63.3 1.8 %copy.17 = f32[2,256,32]{1,2,0:T(8,128)} copy(f32[2,256,32]{2,1,0:T(8,128)} %get-tuple-element.6) | data formatting | bytes 131072 | tf_op jit(solution)/shard_map/pallas_call | solution.py:392
  65.0 1.7 %copy.18 = f32[2,256,32]{1,2,0:T(8,128)} copy(f32[2,256,32]{2,1,0:T(8,128)} %get-tuple-element.7) | data formatting | bytes 131072 | tf_op jit(solution)/shard_map/pallas_call | solution.py:392
  66.7 1.6 %copy.23 = f32[256,128]{1,0:T(8,128)} copy(f32[256,128]{1,0:T(8,128)} %get-tuple-element.20) | data formatting | bytes 262144
  68.3 1.7 %copy.24 = f32[256,256]{1,0:T(8,128)} copy(f32[256,256]{1,0:T(8,128)} %get-tuple-element.21) | data formatting | bytes 524288
  70.0 1.9 %copy.25 = bf16[2048,128]{1,0:T(8,128)(2,1)} copy(bf16[2048,128]{1,0:T(8,128)(2,1)} %get-tuple-element.22) | data formatting | bytes 1048576
  71.8 0.0 copy-done
  71.8 1.0 %copy.26 = bf16[2048,256]{1,0:T(8,128)(2,1)} copy(bf16[2048,256]{1,0:T(8,128)(2,1)S(1)} %copy-done) | data formatting | bytes 2097152
Async XLA Ops:
  63.2 8.6 %copy-start = (bf16[2048,256]{1,0:T(8,128)(2,1)S(1)}, bf16[2048,256]{1,0:T(8,128)(2,1)}, u32[]{:S(2)}) copy-start(bf16[2048,256]{1,0:T(8,128)(2,1)} %get-tuple-element.23) | copy-start | bytes 3145732

commit v2 on v1

--- a/solution.py
+++ b/solution.py
@@ -23,49 +23,22 @@
     return jnp.transpose(a.astype(F32))
 
 
-def kernel(
-    n_fs,
-    n_tp,
-    x_hbm,
-    dk_ref,
-    dv_ref,
-    kf_ref,
-    vf_ref,
-    wk_ref,
-    wv_ref,
-    fm_ref,
-    sm_ref,
-    first_ref,
-    second_ref,
-    newk_ref,
-    newv_ref,
-    kcopy_ref,
-    vcopy_ref,
-    x_ref,
-    part_ref,
-    partin_ref,
-    tok_ref,
-    tokin_ref,
-    sq_ref,
-    sqin_ref,
-    gat_ref,
-    wall_ref,
-    x_sem,
-    part_ss,
-    part_rs,
-    tok_ss,
-    tok_rs,
-    sq_ss,
-    sq_rs,
-    gf_ss,
-    gf_rs,
-    gt_ss,
-    gt_rs,
-    w_ss,
-    w_rs,
-    wx_ss,
-    wx_rs,
-):
+def start(c):
+    c.start()
+
+
+def finish(c):
+    c.wait_send()
+
+
+def kernel(n_fs, n_tp, *refs):
+    hbm = refs[:9]
+    gat_ref, wall_ref, first_ref, second_ref = refs[9:13]
+    held_in = refs[13:22]
+    x_ref, dk_ref, dv_ref, kf_ref, vf_ref, wk_ref, wv_ref, fm_ref, sm_ref = held_in
+    part_ref, partin_ref, tok_ref, tokin_ref, sq_ref, sqin_ref = refs[22:28]
+    in_sem, part_ss, part_rs, tok_ss, tok_rs, sq_ss, sq_rs = refs[28:35]
+    gf_ss, gf_rs, gt_ss, gt_rs, w_ss, w_rs, wx_ss, wx_rs = refs[35:]
     fs = lax.axis_index("fs")
     tp = lax.axis_index("tp")
     n_dev = n_fs * n_tp
@@ -81,8 +54,11 @@
     far = fs // pair
     near = fs % pair
 
-    x_copy = pltpu.make_async_copy(x_hbm, x_ref, x_sem)
-    x_copy.start()
+    loads = [
+        pltpu.make_async_copy(hbm[i], held_in[i], in_sem.at[i]) for i in range(9)
+    ]
+    for i in (3, 4, 1, 2, 5, 6, 0, 7, 8):
+        loads[i].start()
 
     barrier = pltpu.get_barrier_semaphore()
 
@@ -96,6 +72,8 @@
             device_id_type=MESH,
         )
 
+    for i in (3, 4, 1, 2):
+        loads[i].wait()
     kft = flip(kf_ref[...]).astype(BF16)
     vft = flip(vf_ref[...]).astype(BF16)
     last = (((1,), (1,)), ((), ()))
@@ -104,6 +82,8 @@
     for j in range(n_tp):
         part_ref[j, :r, :] = red_k[j * r : (j + 1) * r].astype(BF16)
         part_ref[j, r:, :] = red_v[j * r : (j + 1) * r].astype(BF16)
+    for i in (5, 6):
+        loads[i].wait()
     wall_ref[fs, :, :nk] = wk_ref[...].astype(BF16)
     wall_ref[fs, :, nk:] = wv_ref[...].astype(BF16)
 
@@ -124,44 +104,55 @@
     for c in parts:
         c.start()
 
-    def wall_copy(k):
-        to = lax.rem(far + k, n_far) * pair + near
-        return pltpu.make_async_remote_copy(
-            src_ref=wall_ref.at[fs],
-            dst_ref=wall_ref.at[fs],
-            send_sem=w_ss.at[k - 1],
-            recv_sem=w_rs.at[k - 1],
-            device_id={"fs": to},
-            device_id_type=MESH,
-        )
-
-    def wall_in(k):
-        origin = lax.rem(far + n_far - k, n_far) * pair + near
-        return pltpu.make_async_copy(
-            wall_ref.at[origin], wall_ref.at[origin], w_rs.at[k - 1]
-        )
-
-    def wall_pair(k):
-        block = lax.rem(far + n_far - k, n_far) * pair + near
-        return pltpu.make_async_remote_copy(
-            src_ref=wall_ref.at[block],
-            dst_ref=wall_ref.at[block],
-            send_sem=wx_ss.at[k],
-            recv_sem=wx_rs.at[k],
+    def wall_hop(block_far, way):
+        block = wall_ref.at[block_far * pair + near]
+        return pltpu.make_async_remote_copy(
+            src_ref=block,
+            dst_ref=block,
+            send_sem=w_ss.at[(way + 1) // 2, block_far],
+            recv_sem=w_rs.at[block_far],
+            device_id={"fs": (far + way) * pair + near},
+            device_id_type=MESH,
+        )
+
+    def wall_pair(block_far):
+        block = wall_ref.at[block_far * pair + near]
+        return pltpu.make_async_remote_copy(
+            src_ref=block,
+            dst_ref=block,
+            send_sem=wx_ss.at[block_far],
+            recv_sem=wx_rs.at[block_far],
             device_id={"fs": far * pair + 1 - near},
             device_id_type=MESH,
         )
 
-    walls = [wall_copy(k) for k in range(1, n_far)]
-    for c in walls:
-        c.start()
-    pairs = []
-    if pair == 2:
-        pairs.append(wall_pair(0))
-        pairs[-1].start()
-
-    fmt = jnp.concatenate([flip(fm_ref[0]), flip(fm_ref[1])], axis=0)
-    smt = jnp.concatenate([flip(sm_ref[0]), flip(sm_ref[1])], axis=0)
+    def wall_step(d, act):
+        for way in (1, -1):
+            block_far = far - d * way
+            here = (block_far >= 0) & (block_far < n_far)
+            more = here & (far + way >= 0) & (far + way < n_far)
+            if d == 0:
+                if pair == 2 and way == 1:
+                    act(wall_pair(far))
+            else:
+
+                @pl.when(here)
+                def _():
+                    block = wall_ref.at[block_far * pair + near]
+                    if act is start:
+                        pltpu.make_async_copy(block, block, w_rs.at[block_far]).wait()
+
+            @pl.when(more)
+            def _():
+                act(wall_hop(block_far, way))
+
+            if d and pair == 2:
+
+                @pl.when(here)
+                def _():
+                    act(wall_pair(block_far))
+
+    wall_step(0, start)
 
     for c in parts:
         c.wait_recv()
@@ -169,7 +160,7 @@
     for k in range(1, n_tp):
         own = own + partin_ref[k - 1].astype(F32)
     own = own.astype(BF16)
-    x_copy.wait()
+    loads[0].wait()
 
     def tok_copy(c):
         return pltpu.make_async_remote_copy(
@@ -197,6 +188,13 @@
             def _():
                 tok_copy(c).start()
 
+    if n_far > 1:
+        wall_step(1, start)
+    for i in (7, 8):
+        loads[i].wait()
+    fmt = fm_ref[...].reshape(2 * r, rows)
+    smt = sm_ref[...].reshape(2 * r, rows)
+
     total = tok_ref[fs].astype(F32)
     for k in range(1, n_fs):
         origin = lax.rem(fs + k, n_fs)
@@ -222,6 +220,8 @@
     def _(k):
         sq_copy(k).start()
 
+    if n_far > 2:
+        wall_step(2, start)
     pltpu.make_async_copy(sqin_ref, sqin_ref, sq_rs).wait()
     total_sq = jnp.max(jnp.sum(sqin_ref[...], axis=0) + sq_ref[...])
     limit = clip_target * (2.0 * model * rank) ** 0.5
@@ -313,15 +313,11 @@
     for c in gats:
         c.start()
 
-    for i in range(2):
-        first_ref[i] = jnp.transpose(first_new[i * r : (i + 1) * r])
-        second_ref[i] = jnp.transpose(second_new[i * r : (i + 1) * r])
-
-    for k in range(1, n_far):
-        wall_in(k).wait()
-        if pair == 2:
-            pairs.append(wall_pair(k))
-            pairs[-1].start()
+    first_ref[...] = first_new.reshape(2, r, rows)
+    second_ref[...] = second_new.reshape(2, r, rows)
+
+    for d in range(3, n_far):
+        wall_step(d, start)
 
     order = list(range(n_fs))
     for k in order:
@@ -335,18 +331,65 @@
                 share_in(k, mask | bits[step - 1]).wait()
             share(k, step)
 
+    for k in order:
+        if bits:
+            for mask in sources(len(bits) - 1):
+                share_in(k, mask | bits[-1]).wait()
+    if pair == 2:
+        for m in range(n_far):
+            block = wall_ref.at[m * pair + 1 - near]
+            pltpu.make_async_copy(block, block, wx_rs.at[m]).wait()
+
+    for c in parts + gats + shares:
+        c.wait_send()
+    for d in range(n_far):
+        wall_step(d, finish)
+    for c in range(n_fs):
+
+        @pl.when(c != fs)
+        def _():
+            tok_copy(c).wait_send()
+
+    pltpu.make_async_copy(sqin_ref, sqin_ref, sq_ss).wait()
+
+
+def results(
+    n_fs,
+    gat_ref,
+    wall_ref,
+    first_in,
+    second_in,
+    kf_ref,
+    vf_ref,
+    wk_ref,
+    wv_ref,
+    first_ref,
+    second_ref,
+    newk_ref,
+    newv_ref,
+    kout_ref,
+    vout_ref,
+    kcopy_ref,
+    vcopy_ref,
+    k_sem,
+    v_sem,
+):
+    fs = lax.axis_index("fs")
+    rows, nk = wk_ref.shape
     back = (((0,), (0,)), ((), ()))
+    kft = flip(kf_ref[...]).astype(BF16)
+    vft = flip(vf_ref[...]).astype(BF16)
+    first_ref[...] = first_in[...]
+    second_ref[...] = second_in[...]
 
     def update(block):
         up_k = lax.dot_general(gat_ref[block, 0], kft, back, preferred_element_type=F32)
         up_v = lax.dot_general(gat_ref[block, 1], vft, back, preferred_element_type=F32)
         return step_rate * up_k, step_rate * up_v
 
+    outs = []
     for k in range(n_fs):
-        origin = lax.rem(fs + n_fs - k, n_fs)
-        if bits:
-            for mask in sources(len(bits) - 1):
-                share_in(k, mask | bits[-1]).wait()
+        origin = lax.rem(fs + k, n_fs)
         up_k, up_v = update(origin)
         at = pl.ds(pl.multiple_of(origin * rows, rows), rows)
         if k == 0:
@@ -354,31 +397,22 @@
             new_v = wv_ref[...] - up_v
             newk_ref[...] = new_k
             newv_ref[...] = new_v
-            kcopy_ref[at, :] = new_k.astype(BF16)
-            vcopy_ref[at, :] = new_v.astype(BF16)
         else:
-            if k == 1:
-                for m in range(n_far if pair == 2 else 0):
-                    block = lax.rem(far + n_far - m, n_far) * pair + 1 - near
-                    pltpu.make_async_copy(
-                        wall_ref.at[block], wall_ref.at[block], wx_rs.at[m]
-                    ).wait()
-            kcopy_ref[at, :] = (wall_ref[origin, :, :nk].astype(F32) - up_k).astype(BF16)
-            vcopy_ref[at, :] = (wall_ref[origin, :, nk:].astype(F32) - up_v).astype(BF16)
-
-    for c in parts + walls + pairs + gats + shares:
-        c.wait_send()
-    for c in range(n_fs):
-
-        @pl.when(c != fs)
-        def _():
-            tok_copy(c).wait_send()
-
-    pltpu.make_async_copy(sqin_ref, sqin_ref, sq_ss).wait()
-
-
-def local(n_fs, n_tp, *args):
-    x, dk, dv, kf, vf, wk, wv, fm, sm = args
+            new_k = wall_ref[origin, :, :nk].astype(F32) - up_k
+            new_v = wall_ref[origin, :, nk:].astype(F32) - up_v
+        kcopy_ref[k] = new_k.astype(BF16)
+        vcopy_ref[k] = new_v.astype(BF16)
+        for c in (
+            pltpu.make_async_copy(kcopy_ref.at[k], kout_ref.at[at, :], k_sem.at[k]),
+            pltpu.make_async_copy(vcopy_ref.at[k], vout_ref.at[at, :], v_sem.at[k]),
+        ):
+            c.start()
+            outs.append(c)
+    for c in outs:
+        c.wait()
+
+
+def local(n_fs, n_tp, x, dk, dv, kf, vf, wk, wv, fm, sm):
     tokens, model = x.shape
     rows, nk = wk.shape
     nv = wv.shape[1]
@@ -387,33 +421,33 @@
     n_dev = n_fs * n_tp
     dma = pltpu.SemaphoreType.DMA
     vmem = pl.BlockSpec(memory_space=pltpu.VMEM)
+    anywhere = pl.BlockSpec(memory_space=pl.ANY)
     pair = 2 if n_fs % 2 == 0 else 1
     n_far = n_fs // pair
-    return pl.pallas_call(
+    peers = max(n_tp - 1, 1)
+    args = (x, dk, dv, kf, vf, wk, wv, jnp.swapaxes(fm, 1, 2), jnp.swapaxes(sm, 1, 2))
+    placed = [pltpu.with_memory_space_constraint(a, pltpu.HBM) for a in args]
+    gat, wall, first, second = pl.pallas_call(
         functools.partial(kernel, n_fs, n_tp),
         out_shape=(
-            jax.ShapeDtypeStruct(fm.shape, F32),
-            jax.ShapeDtypeStruct(sm.shape, F32),
-            jax.ShapeDtypeStruct(wk.shape, F32),
-            jax.ShapeDtypeStruct(wv.shape, F32),
-            jax.ShapeDtypeStruct((model, nk), BF16),
-            jax.ShapeDtypeStruct((model, nv), BF16),
+            pltpu.VMEM((n_fs, 2, rank, rows), BF16),
+            pltpu.VMEM((n_fs, rows, nk + nv), BF16),
+            pltpu.VMEM((2, r, rows), F32),
+            pltpu.VMEM((2, r, rows), F32),
         ),
-        in_specs=[pl.BlockSpec(memory_space=pl.ANY)] + [vmem] * 8,
-        out_specs=(vmem,) * 6,
-        scratch_shapes=[
-            pltpu.VMEM((tokens, model), BF16),
+        in_specs=[pl.BlockSpec(memory_space=pltpu.HBM)] * 9,
+        out_specs=(vmem,) * 4,
+        scratch_shapes=[pltpu.VMEM(a.shape, a.dtype) for a in args]
+        + [
             pltpu.VMEM((n_tp, 2 * r, tokens), BF16),
-            pltpu.VMEM((max(n_tp - 1, 1), 2 * r, tokens), BF16),
+            pltpu.VMEM((peers, 2 * r, tokens), BF16),
             pltpu.VMEM((n_fs, 2 * r, rows), BF16),
             pltpu.VMEM((n_fs, 2 * r, rows), BF16),
             pltpu.VMEM((8, 128), F32),
             pltpu.VMEM((n_dev - 1, 8, 128), F32),
-            pltpu.VMEM((n_fs, 2, rank, rows), BF16),
-            pltpu.VMEM((n_fs, rows, nk + nv), BF16),
-            dma,
-            dma((max(n_tp - 1, 1),)),
-            dma((max(n_tp - 1, 1),)),
+            dma((9,)),
+            dma((peers,)),
+            dma((peers,)),
             dma((n_fs,)),
             dma((n_fs,)),
             dma,
@@ -422,15 +456,43 @@
             dma((n_fs,)),
             dma((n_fs, n_tp)),
             dma((n_fs, n_tp)),
-            dma((n_far,)),
+            dma((2, n_far)),
             dma((n_far,)),
             dma((n_far,)),
             dma((n_far,)),
         ],
         compiler_params=pltpu.CompilerParams(
-            collective_id=0, has_side_effects=True, vmem_limit_bytes=60 * 1024 * 1024
+            collective_id=0, has_side_effects=True, vmem_limit_bytes=40 * 1024 * 1024
         ),
-    )(*args)
+    )(*placed)
+    first, second, new_k, new_v, k_copy, v_copy = pl.pallas_call(
+        functools.partial(results, n_fs),
+        out_shape=(
+            jax.ShapeDtypeStruct(first.shape, F32),
+            jax.ShapeDtypeStruct(second.shape, F32),
+            jax.ShapeDtypeStruct(wk.shape, F32),
+            jax.ShapeDtypeStruct(wv.shape, F32),
+            jax.ShapeDtypeStruct((model, nk), BF16),
+            jax.ShapeDtypeStruct((model, nv), BF16),
+        ),
+        in_specs=[vmem] * 8,
+        out_specs=(vmem,) * 4 + (anywhere,) * 2,
+        scratch_shapes=[
+            pltpu.VMEM((n_fs, rows, nk), BF16),
+            pltpu.VMEM((n_fs, rows, nv), BF16),
+            dma((n_fs,)),
+            dma((n_fs,)),
+        ],
+        compiler_params=pltpu.CompilerParams(vmem_limit_bytes=32 * 1024 * 1024),
+    )(gat, wall, first, second, kf, vf, wk, wv)
+    return (
+        jnp.swapaxes(first, 1, 2),
+        jnp.swapaxes(second, 1, 2),
+        new_k,
+        new_v,
+        k_copy,
+        v_copy,
+    )
 
 
 def solution(mesh):

time: 73.2 us -> 46.2 us (0.63)
  Pallas kernels: 59.3 us -> 45.3 us
  local copies, waits for them, and re-layouts: 12.9 us -> 0.02 us
    pallas_call x1 -> x2, Pallas kernels: 59.3 us -> 45.3 us  [the longest x1 42.9 us: local(): pl.pallas_call(functools.partial(kernel, n_fs, n_tp), out_shape=(pltpu.VM...]
    unnamed x8, local copies, waits for them, and re-layouts: 9.43 us -> 0.02 us
    pallas_call x2 -> x0, local copies, waits for them, and re-layouts: 3.46 us -> none  [local(): pl.pallas_call(functools.partial(kernel, n_fs, n_tp), out_shape=(jax.Shap...]
where the time goes in v2:
time: 46.2 us; the launch traced here: 46.1 us
  Pallas kernels  45.3 us (98%)
  between operations  0.71 us (2%)
    pallas_call x1, Pallas kernels, local(): pl.pallas_call(functools.partial(kernel, n_fs, n_tp), out_shape=(pltpu.VM...  42.9 us
    pallas_call x1, Pallas kernels, local(): pl.pallas_call(functools.partial(results, n_fs), out_shape=(jax.ShapeDtyp...  2.39 us

profile of v2, /device:TPU:0, one launch (start us, length us, event | category | flops | bytes accessed | tf_op | source)
XLA Modules:
  0.0 46.1 jit_solution(12320715385813381119)
XLA Ops:
  0.6 0.0 copy-start
  0.6 0.0 copy-start.1
  0.7 0.0 copy-start.2
  0.7 0.0 copy-start.3
  0.7 42.9 %shard_map.136 = (bf16[8,2,128,256]{3,2,1,0:T(8,128)(2,1)S(1)}, bf16[8,256,384]{2,1,0:T(8,128)(2,1)S(1)}, f32[2,32,256]{2,1,0:T(8,128)S(1)}, f32[2,32,256]{2,1,0:T(8,128)S(1)}) custom-call(bf16[640,2048]{1,0:T(8,128)(2,1)} %refs_0_.1, bf16[640,128]{1,0:T(8,128)(2,1)} %refs_1_.1, bf16[640,256]{1,0:T(8,128)(2,1)} %refs_2_.1, bf16[128,128]{1,0:T(8,128)(2,1)} %kf_ref.1, ...), custom_call_target="tpu_custom_call" | custom-call | tf_op jit(solution)/shard_map/pallas_call | solution.py:430
  43.6 0.0 copy-done
  43.6 0.0 copy-done.1
  43.6 0.0 copy-done.2
  43.7 0.0 copy-done.3
  43.7 2.4 %shard_map.137 = (f32[2,32,256]{2,1,0:T(8,128)}, f32[2,32,256]{2,1,0:T(8,128)}, f32[256,128]{1,0:T(8,128)}, f32[256,256]{1,0:T(8,128)}, bf16[2048,128]{1,0:T(8,128)(2,1)}, /*index=5*/bf16[2048,256]{1,0:T(8,128)(2,1)}) custom-call(bf16[8,2,128,256]{3,2,1,0:T(8,128)(2,1)S(1)} %get-tuple-element.16.gat_ref, ...), custom_call_target="tpu_custom_call" | custom-call | tf_op jit(solution)/shard_map/pallas_call | solution.py:468
Async XLA Ops:
  0.6 43.0 %copy-start = (f32[256,256]{1,0:T(8,128)S(1)}, f32[256,256]{1,0:T(8,128)}, u32[]{:S(2)}) copy-start(f32[256,256]{1,0:T(8,128)} %wv_ref.1) | copy-start | bytes 786436
  0.6 43.0 %copy-start.1 = (f32[256,128]{1,0:T(8,128)S(1)}, f32[256,128]{1,0:T(8,128)}, u32[]{:S(2)}) copy-start(f32[256,128]{1,0:T(8,128)} %wk_ref.1) | copy-start | bytes 393220
  0.7 43.0 %copy-start.2 = (bf16[256,128]{1,0:T(8,128)(2,1)S(1)}, bf16[256,128]{1,0:T(8,128)(2,1)}, u32[]{:S(2)}) copy-start(bf16[256,128]{1,0:T(8,128)(2,1)} %vf_ref.1) | copy-start | bytes 196612
  0.7 43.0 %copy-start.3 = (bf16[128,128]{1,0:T(8,128)(2,1)S(1)}, bf16[128,128]{1,0:T(8,128)(2,1)}, u32[]{:S(2)}) copy-start(bf16[128,128]{1,0:T(8,128)(2,1)} %kf_ref.1) | copy-start | bytes 98308

commit v3 on v2

--- a/solution.py
+++ b/solution.py
@@ -301,15 +301,14 @@
 
     shares = []
 
-    def share(k, step):
-        for mask in sources(step):
-            c = share_copy(k, step, mask)
-            c.start()
-            shares.append(c)
+    def share(k, step, mask):
+        c = share_copy(k, step, mask)
+        c.start()
+        shares.append(c)
 
     gats = [gat_copy(k) for k in range(1, n_fs)]
-    if bits:
-        share(0, 0)
+    for step in range(len(bits)):
+        share(0, step, 0)
     for c in gats:
         c.start()
 
@@ -323,14 +322,15 @@
     for k in order:
         if k:
             gat_in(k).wait()
-            if bits:
-                share(k, 0)
+            for step in range(len(bits)):
+                share(k, step, 0)
     for step in range(1, len(bits)):
         for k in order:
             for mask in sources(step - 1):
-                share_in(k, mask | bits[step - 1]).wait()
-            share(k, step)
-
+                got = mask | bits[step - 1]
+                share_in(k, got).wait()
+                for later in range(step, len(bits)):
+                    share(k, later, got)
     for k in order:
         if bits:
             for mask in sources(len(bits) - 1):
@@ -443,8 +443,8 @@
             pltpu.VMEM((peers, 2 * r, tokens), BF16),
             pltpu.VMEM((n_fs, 2 * r, rows), BF16),
             pltpu.VMEM((n_fs, 2 * r, rows), BF16),
-            pltpu.VMEM((8, 128), F32),
-            pltpu.VMEM((n_dev - 1, 8, 128), F32),
+            pltpu.VMEM((1, 128), F32),
+            pltpu.VMEM((n_dev - 1, 1, 128), F32),
             dma((9,)),
             dma((peers,)),
             dma((peers,)),

time: 46.2 us -> 44 us (0.952)
  Pallas kernels: 45.3 us -> 43.1 us
    pallas_call x1, Pallas kernels: 42.9 us -> 40.7 us  [local(): pl.pallas_call(functools.partial(kernel, n_fs, n_tp), out_shape=(pltpu.VM...]
where the time goes in v3:
time: 44 us; the launch traced here: 43.9 us
  Pallas kernels  43.1 us (98%)
  between operations  0.71 us (2%)
    pallas_call x1, Pallas kernels, local(): pl.pallas_call(functools.partial(kernel, n_fs, n_tp), out_shape=(pltpu.VM...  40.7 us
    pallas_call x1, Pallas kernels, local(): pl.pallas_call(functools.partial(results, n_fs), out_shape=(jax.ShapeDtyp...  2.39 us

profile of v3, /device:TPU:0, one launch (start us, length us, event | category | flops | bytes accessed | tf_op | source)
XLA Modules:
  0.0 43.9 jit_solution(9452313380187073574)
XLA Ops:
  0.6 0.0 copy-start
  0.6 0.0 copy-start.1
  0.7 0.0 copy-start.2
  0.7 0.0 copy-start.3
  0.7 40.7 %shard_map.136 = (bf16[8,2,128,256]{3,2,1,0:T(8,128)(2,1)S(1)}, bf16[8,256,384]{2,1,0:T(8,128)(2,1)S(1)}, f32[2,32,256]{2,1,0:T(8,128)S(1)}, f32[2,32,256]{2,1,0:T(8,128)S(1)}) custom-call(bf16[640,2048]{1,0:T(8,128)(2,1)} %refs_0_.1, bf16[640,128]{1,0:T(8,128)(2,1)} %refs_1_.1, bf16[640,256]{1,0:T(8,128)(2,1)} %refs_2_.1, bf16[128,128]{1,0:T(8,128)(2,1)} %kf_ref.1, ...), custom_call_target="tpu_custom_call" | custom-call | tf_op jit(solution)/shard_map/pallas_call | solution.py:430
  41.4 0.0 copy-done
  41.4 0.0 copy-done.1
  41.4 0.0 copy-done.2
  41.5 0.0 copy-done.3
  41.5 2.4 %shard_map.137 = (f32[2,32,256]{2,1,0:T(8,128)}, f32[2,32,256]{2,1,0:T(8,128)}, f32[256,128]{1,0:T(8,128)}, f32[256,256]{1,0:T(8,128)}, bf16[2048,128]{1,0:T(8,128)(2,1)}, /*index=5*/bf16[2048,256]{1,0:T(8,128)(2,1)}) custom-call(bf16[8,2,128,256]{3,2,1,0:T(8,128)(2,1)S(1)} %get-tuple-element.16.gat_ref, ...), custom_call_target="tpu_custom_call" | custom-call | tf_op jit(solution)/shard_map/pallas_call | solution.py:468
Async XLA Ops:
  0.6 40.8 %copy-start = (f32[256,256]{1,0:T(8,128)S(1)}, f32[256,256]{1,0:T(8,128)}, u32[]{:S(2)}) copy-start(f32[256,256]{1,0:T(8,128)} %wv_ref.1) | copy-start | bytes 786436
  0.6 40.8 %copy-start.1 = (f32[256,128]{1,0:T(8,128)S(1)}, f32[256,128]{1,0:T(8,128)}, u32[]{:S(2)}) copy-start(f32[256,128]{1,0:T(8,128)} %wk_ref.1) | copy-start | bytes 393220
  0.7 40.8 %copy-start.2 = (bf16[256,128]{1,0:T(8,128)(2,1)S(1)}, bf16[256,128]{1,0:T(8,128)(2,1)}, u32[]{:S(2)}) copy-start(bf16[256,128]{1,0:T(8,128)(2,1)} %vf_ref.1) | copy-start | bytes 196612
  0.7 40.8 %copy-start.3 = (bf16[128,128]{1,0:T(8,128)(2,1)S(1)}, bf16[128,128]{1,0:T(8,128)(2,1)}, u32[]{:S(2)}) copy-start(bf16[128,128]{1,0:T(8,128)(2,1)} %kf_ref.1) | copy-start | bytes 98308
